TPU v7x, 32 devices: a whole 2x2x4 slice. The times are simulated.
32 devices in a mesh: fs: 8 (over z, x), tp: 4 (over y, core).
Axes of the slice: x: 2, y: 2, z: 4, core: 2. Of those that a mesh axis runs over, the one named last changes fastest.
Arguments:
- inputs: bfloat16 [3072, 2048], P('fs'), may hold values from -6 to 6
- queries: bfloat16 [3072, 2048], P('fs', 'tp'), may hold values from -6 to 6
- keys: bfloat16 [3072, 2048], P('fs', 'tp'), may hold values from -6 to 6
- values: bfloat16 [3072, 2048], P('fs', 'tp'), may hold values from -6 to 6
- head_cot: bfloat16 [3072, 2048], P('fs', 'tp'), may hold values from -6 to 6
- mixing: float32 [16], P('tp'), may hold values from 0.3 to 0.8
- head_gain: float32 [128], replicated, may hold values from 0.1 to 1.9
- factors: bfloat16 [2048, 2, 256], P('fs'), may hold values from -0.375 to 0.375
- moments: float32 [256, 2, 2048], P('fs', None, 'tp'), may hold values from -6 to 6
- weights: float32 [2048, 2, 2048], P('fs', None, 'tp'), may hold values from -6 to 6
Outputs:
- step: float32 [2048, 2, 2048], P('fs', None, 'tp')
- new_moments: float32 [256, 2, 2048], P('fs', None, 'tp')
- copies: bfloat16 [2048, 2, 2048], P(None, None, 'tp')
All inputs are finite; a program needn't handle non-finite values.
Results may differ from a plain program's by a relative error of at most 0.007.
Values may be sent and summed in bfloat16 or wider, within the bound.
A program may use at most 64 MiB of HBM per device.

v0:
```python
import jax
import jax.numpy as jnp
from jax import lax
from jax.sharding import PartitionSpec as P

EPS = 0.05
BETA = 0.9
RATE_BASE = 0.5


def softmax_rows(scores):
    top = jnp.max(scores, axis=-1, keepdims=True)
    expo = jnp.exp(scores - top)
    return expo / jnp.sum(expo, axis=-1, keepdims=True)


def head_grads(query, key_rows, value, upstream, weight_mix, head_gain):
    length = query.shape[0]
    head_dim = query.shape[2]
    factor = head_dim ** (-0.5)
    places = jnp.arange(length)
    causal = places[None, :] <= places[:, None]

    def probs(which):
        scores = (
            jnp.dot(query[:, which], key_rows[:, which].T, preferred_element_type=jnp.float32)
            * factor
        )
        return softmax_rows(jnp.where(causal, scores, -jnp.inf))

    first = probs(0)
    second = probs(1)
    mixed = (first - weight_mix * second).astype(jnp.bfloat16)
    output = jnp.dot(mixed, value, preferred_element_type=jnp.float32)
    inverse = lax.rsqrt(jnp.mean(output * output, axis=-1, keepdims=True) + EPS)
    scaled = head_gain * upstream.astype(jnp.float32)
    d_out = inverse * scaled - output * inverse**3 * jnp.mean(
        output * scaled, axis=-1, keepdims=True
    )
    d_out = d_out.astype(jnp.bfloat16)
    d_value = jnp.dot(mixed.T, d_out, preferred_element_type=jnp.float32).astype(jnp.bfloat16)
    d_mix = jnp.dot(d_out, value.T, preferred_element_type=jnp.float32)
    d_first = (first * (d_mix - jnp.sum(first * d_mix, axis=-1, keepdims=True))).astype(
        jnp.bfloat16
    )
    d_second = (
        -weight_mix * second * (d_mix - jnp.sum(second * d_mix, axis=-1, keepdims=True))
    ).astype(jnp.bfloat16)
    q_first = (
        jnp.dot(d_first, key_rows[:, 0], preferred_element_type=jnp.float32) * factor
    ).astype(jnp.bfloat16)
    q_second = (
        jnp.dot(d_second, key_rows[:, 1], preferred_element_type=jnp.float32) * factor
    ).astype(jnp.bfloat16)
    return (jnp.stack([q_first, q_second], axis=1).reshape(length, 2 * head_dim), d_value)


def per_device(
    inputs, queries, keys, values, head_cot, mixing, head_gain, factors, moments, weights
):
    length = inputs.shape[0]
    heads_here = mixing.shape[0]
    head_width = values.shape[1] // heads_here
    head_dim = head_width // 2
    query_heads = queries.reshape(length, heads_here, 2, head_dim).transpose(1, 0, 2, 3)
    key_heads = keys.reshape(length, heads_here, 2, head_dim).transpose(1, 0, 2, 3)
    value_heads = values.reshape(length, heads_here, head_width).transpose(1, 0, 2)
    upstream_heads = head_cot.reshape(length, heads_here, head_width).transpose(1, 0, 2)

    def one_head(pieces):
        return head_grads(pieces[0], pieces[1], pieces[2], pieces[3], pieces[4], head_gain)

    d_query, d_value = lax.map(
        one_head, (query_heads, key_heads, value_heads, upstream_heads, mixing)
    )
    d_query = d_query.transpose(1, 0, 2).reshape(length, heads_here * head_width)
    d_value = d_value.transpose(1, 0, 2).reshape(length, heads_here * head_width)
    cotangents = jnp.stack([d_query, d_value], axis=1)
    fs_count = lax.axis_size("fs")
    token_factor = (length * fs_count) ** (-0.5)
    rank_here = moments.shape[0]
    cols_here = moments.shape[2]
    factor_wide = factors.astype(jnp.float32)
    whole_factors = lax.all_gather(factors, "fs", axis=0, tiled=True)
    reduced = jnp.einsum("td,dkr->tkr", inputs, whole_factors, preferred_element_type=jnp.float32)
    reduced_upper = reduced.astype(jnp.bfloat16)
    reduced_lower = (reduced - reduced_upper.astype(jnp.float32)).astype(jnp.bfloat16)
    upper_part = jnp.einsum(
        "tkr,tke->rke", reduced_upper, cotangents, preferred_element_type=jnp.float32
    )
    lower_part = jnp.einsum(
        "tkr,tke->rke", reduced_lower, cotangents, preferred_element_type=jnp.float32
    )
    projected = lax.psum_scatter(upper_part + lower_part, "fs", scatter_dimension=0, tiled=True)
    projected = projected * token_factor
    new_moments = BETA * moments + projected
    local_sums = jnp.sum(new_moments * new_moments, axis=(0, 2))
    totals = lax.psum(local_sums, ("fs", "tp"))
    entries = rank_here * fs_count * cols_here * lax.axis_size("tp")
    rate = RATE_BASE / jnp.sqrt(1.0 + totals / entries)
    low_part = jnp.einsum(
        "dkr,rke->dke",
        factor_wide,
        lax.all_gather(new_moments, "fs", axis=0, tiled=True),
        precision=lax.Precision.HIGHEST,
    )
    step = low_part * rate[None, :, None]
    copies = lax.all_gather((weights - step).astype(jnp.bfloat16), "fs", axis=0, tiled=True)
    return (step, new_moments, copies)


def solution(mesh):
    placed = (
        P("fs", None),
        P("fs", "tp"),
        P("fs", "tp"),
        P("fs", "tp"),
        P("fs", "tp"),
        P("tp"),
        P(),
        P("fs", None, None),
        P("fs", None, "tp"),
        P("fs", None, "tp"),
    )
    return jax.shard_map(
        per_device,
        mesh=mesh,
        in_specs=placed,
        out_specs=(P("fs", None, "tp"), P("fs", None, "tp"), P(None, None, "tp")),
        check_vma=False,
    )
```

profile of v0, /device:TPU:0, one launch (start us, length us, event | category | flops | bytes accessed | tf_op | source)
XLA Modules:
  0.0 282.7 jit_solution(10454785109164463003)
XLA Ops:
  7.3 1.8 copy.46
  9.2 1.2 copy.39
  10.4 1.2 copy.40
  11.8 1.2 copy.42
  13.0 21.3 %while.12 = (s32[]{:T(128)}, bf16[4,384,128]{1,2,0:T(8,128)(2,1)S(1)}, bf16[4,384,128]{2,1,0:T(8,128)(2,1)}, bf16[4,384,2,64]{1,3,2,0:T(8,128)(2,1)S(1)}, bf16[4...) while((s32[]{:T(128)}, ...), condition=%wide.region_9.10_spmd, body=%wide.region_0.9_spmd.sunk | while | flops 195525504 | bytes 10978449 | solution.py:73
  13.1 0.6 dynamic_slice.47
  15.2 0.8 subtract_convert_fusion.5
  16.3 1.0 fusion.71
  18.4 0.6 dynamic_slice.47
  20.5 0.8 subtract_convert_fusion.5
  21.6 1.0 fusion.71
  23.7 0.6 dynamic_slice.47
  25.8 0.8 subtract_convert_fusion.5
  26.9 1.0 fusion.71
  29.0 0.6 dynamic_slice.47
  31.2 0.8 subtract_convert_fusion.5
  32.3 1.0 fusion.71
  34.3 1.2 copy.45
  35.6 27.0 %all-gather.4.cloned.1.call-done = bf16[2048,2,256]{2,0,1:T(8,128)(2,1)} async-done(((bf16[256,2,256]{2,0,1:T(8,128)(2,1)}), bf16[2048,2,256]{2,0,1:T(8,128)(2,1)}) %all-gather.4.cloned.1.call-update) | async-done | bytes 2097168 | tf_op jit(solution)/shard_map/all_gather | solution.py:84
  62.6 2.6 fusion.30
  65.2 0.4 fusion.35
  65.6 0.4 fusion.32
  66.1 1.3 copy.47
  67.5 0.6 dynamic-slice
  68.7 75.5 %all-reduce.3.cloned.1.call-done = f32[256,2,512]{2,1,0:T(2,128)} async-done(((f32[256,2,512]{2,1,0:T(2,128)}), f32[256,2,512]{2,1,0:T(2,128)}) %all-reduce.3.cloned.1.call-update) | async-done | bytes 1048592
  144.3 1.8 multiply_reduce_fusion.3
  146.1 1.4 copy.50
  147.6 39.7 %psum.7 = f32[2]{0:T(128)S(1)} all-reduce(f32[2]{0:T(128)S(1)} %get-tuple-element.111), channel_id=1, replica_groups=mesh['fs'=8,'tp'=4] {'fs','tp'}, use_global_device_ids=true, to_apply=%region_12.13 | all-reduce | flops 2 | bytes 16 | tf_op jit(solution)/shard_map/psum | solution.py:98
  187.3 3.5 %subtract_convert_fusion.1 = (bf16[256,2,512]{0,2,1:T(8,128)(2,1)}, f32[256,2,512]{0,2,1:T(8,128)S(1)}) fusion(f32[256,2,512]{0,2,1:T(8,128)} %copy.50, f32[2]{0:T(128)S(1)} %rsqrt_multiply_fusion, bf16[256,2,256]{2,1,0:T(2,128)(2,1)S(1)} %copy-done.1, f32[256,2,512]{2,1,0:T(2,128)} %all-gather.6.cloned.1.call-done), kind=kOutput, calls=%fused_computation.61 | convolution fusion | flops 806092800 | bytes 3932168 | tf_op jit(solution)/shard_map/dkr,rke->dke/dot_general | solution.py:101
  190.8 1.3 copy.51
  192.1 72.9 %all-gather.8.cloned.1.call-done = bf16[2048,2,512]{0,2,1:T(8,128)(2,1)} async-done(((bf16[256,2,512]{0,2,1:T(8,128)(2,1)}), bf16[2048,2,512]{0,2,1:T(8,128)(2,1)}) %all-gather.8.cloned.1.call-update) | async-done | bytes 4194320 | tf_op jit(solution)/shard_map/all_gather | solution.py:108
  265.0 11.1 %copy.52 = bf16[2048,2,512]{2,1,0:T(2,128)(2,1)} copy(bf16[2048,2,512]{0,2,1:T(8,128)(2,1)} %all-gather.8.cloned.1.call-done) | data formatting | bytes 8388608
  (81 shorter events, 9.3 us)
Async XLA Ops:
  7.2 55.4 %copy-start = (bf16[384,2048]{1,0:T(8,128)(2,1)S(1)}, bf16[384,2048]{1,0:T(8,128)(2,1)}, u32[]{:S(2)}) copy-start(bf16[384,2048]{1,0:T(8,128)(2,1)} %param.12) | copy-start | bytes 4718596
  7.2 4.4 %copy-start.3 = (bf16[384,512]{1,0:T(8,128)(2,1)S(1)}, bf16[384,512]{1,0:T(8,128)(2,1)}, u32[]{:S(2)}) copy-start(bf16[384,512]{1,0:T(8,128)(2,1)} %param.15) | copy-start | bytes 1179652
  7.2 5.8 %copy-start.5 = (f32[128]{0:T(128)S(1)}, f32[128]{0:T(128)}, u32[]{:S(2)}) copy-start(f32[128]{0:T(128)} %param.18) | copy-start | bytes 1540
  7.2 5.8 %copy-start.6 = (f32[4]{0:T(128)S(1)}, f32[4]{0:T(128)}, u32[]{:S(2)}) copy-start(f32[4]{0:T(128)} %param.17) | copy-start | bytes 52
  7.2 55.4 %all-gather.4.cloned.1.call-start = ((), (), s32[]{:S(2)}) async-start(), calls=%async_computation | async-start | bytes 2359296 | tf_op jit(solution)/shard_map/all_gather | solution.py:84
  9.1 135.2 %all-reduce.3.cloned.1.call-start = ((), (), s32[]{:S(2)}) async-start(), calls=%async_computation.3 | async-start | bytes 2097152
  66.1 1.4 copy-start.7
  66.1 78.2 %copy-start.4 = (f32[32,2,512]{2,1,0:T(2,128)S(1)}, f32[32,2,512]{2,1,0:T(2,128)}, u32[]{:S(2)}) copy-start(f32[32,2,512]{2,1,0:T(2,128)} %param.20) | copy-start | bytes 393220
  67.4 78.8 %copy-start.2 = (f32[256,2,512]{2,1,0:T(2,128)S(1)}, f32[256,2,512]{2,1,0:T(2,128)}, u32[]{:S(2)}) copy-start(f32[256,2,512]{2,1,0:T(2,128)} %param.21) | copy-start | bytes 3145732
  67.4 119.9 %copy-start.1 = (bf16[256,2,256]{2,1,0:T(2,128)(2,1)S(1)}, bf16[256,2,256]{2,1,0:T(2,128)(2,1)}, u32[]{:S(2)}) copy-start(bf16[256,2,256]{2,1,0:T(2,128)(2,1)} %param.19) | copy-start | bytes 786436
  67.4 119.9 %all-gather.6.cloned.1.call-start = ((), (), s32[]{:S(2)}) async-start(), calls=%async_computation.1 | async-start | bytes 1179648 | tf_op jit(solution)/shard_map/all_gather | solution.py:104
  146.1 118.9 %all-gather.8.cloned.1.call-start = ((), (), s32[]{:S(2)}) async-start(), calls=%async_computation.2 | async-start | bytes 4718592 | tf_op jit(solution)/shard_map/all_gather | solution.py:108
Sparse Core Ops, SparseCore 0:
  10.8 51.7 all-gather.3
  67.5 76.6 all-reduce.2
  147.0 40.0 all-gather.5
  190.9 74.0 all-gather.7
where the time goes:
time: 283 us
  waiting for transfers between devices  176 us (62%)
  blocking collectives  39.7 us (14%)
  local copies, waits for them, and re-layouts  25.2 us (9%)
  matrix products  18.3 us (6%)
  between operations  14.6 us (5%)
  other arithmetic  6.28 us (2%)
    unnamed x5, waiting for transfers between devices  75.6 us
    all_gather x1, waiting for transfers between devices, per_device(): lax.all_gather((weights - step).astype(jnp.bfloat16), 'fs', axis=0, tiled...  72.9 us
    psum x1, blocking collectives, per_device(): totals = lax.psum(local_sums, ('fs', 'tp'))  39.7 us
    all_gather x1, waiting for transfers between devices, per_device(): whole_factors = lax.all_gather(factors, 'fs', axis=0, tiled=True)  27 us
    unnamed x25, local copies, waits for them, and re-layouts  20.1 us
  transfers between devices with their start and end apart: 4, of which 3 were waited for; matrix products, arithmetic and copies ran while one was open for 10% of the time, Pallas kernels for 0%

commit v1 on v0

--- a/solution.py
+++ b/solution.py
@@ -81,8 +81,19 @@
     rank_here = moments.shape[0]
     cols_here = moments.shape[2]
     factor_wide = factors.astype(jnp.float32)
-    whole_factors = lax.all_gather(factors, "fs", axis=0, tiled=True)
-    reduced = jnp.einsum("td,dkr->tkr", inputs, whole_factors, preferred_element_type=jnp.float32)
+    size, index, span = (lax.axis_size("fs"), lax.axis_index("fs"), factors.shape[0])
+    right = [(i, (i + 1) % size) for i in range(size)]
+    current, reduced = (factors, None)
+    for k in range(size):
+        coming = lax.ppermute(current, "fs", right) if k < size - 1 else None
+        absorb = jnp.einsum(
+            "td,dkr->tkr",
+            lax.dynamic_slice_in_dim(inputs, (index - k) % size * span, current.shape[0], axis=1),
+            current,
+            preferred_element_type=jnp.float32,
+        )
+        reduced = absorb if reduced is None else reduced + absorb
+        current = coming
     reduced_upper = reduced.astype(jnp.bfloat16)
     reduced_lower = (reduced - reduced_upper.astype(jnp.float32)).astype(jnp.bfloat16)
     upper_part = jnp.einsum(

time: 283 us -> 314 us (1.11)
  waiting for transfers between devices: 176 us -> 200 us
  starting transfers between devices: 0.16 us -> 4.7 us
    ppermute x0 -> x7, waiting for transfers between devices: none -> 52.7 us  [per_device(): coming = lax.ppermute(current, 'fs', right) if k < size - 1 else None]
    all_gather x1 -> x0, waiting for transfers between devices: 27 us -> none  [per_device(): whole_factors = lax.all_gather(factors, 'fs', axis=0, tiled=True)]
    ppermute x0 -> x7, starting transfers between devices: none -> 4.58 us  [per_device(): coming = lax.ppermute(current, 'fs', right) if k < size - 1 else None]
    unnamed x5 -> x4, waiting for transfers between devices: 75.6 us -> 74.4 us
    unnamed x25 -> x29, local copies, waits for them, and re-layouts: 20.1 us -> 19.2 us
  transfers between devices with their start and end apart: 4 -> 10, of which waited for: 3 -> 8; matrix products, arithmetic and copies ran while one was open for 10% -> 10% of each run, Pallas kernels for 0% -> 0%
where the time goes in v1:
time: 314 us
  waiting for transfers between devices  200 us (64%)
  blocking collectives  39.7 us (13%)
  local copies, waits for them, and re-layouts  26.9 us (9%)
  matrix products  18.8 us (6%)
  between operations  14.7 us (5%)
  other arithmetic  6.25 us (2%)
  starting transfers between devices  4.7 us (1%)
    unnamed x4, waiting for transfers between devices  74.4 us
    all_gather x1, waiting for transfers between devices, per_device(): lax.all_gather((weights - step).astype(jnp.bfloat16), 'fs', axis=0, tiled...  72.9 us
    ppermute x7, waiting for transfers between devices, per_device(): coming = lax.ppermute(current, 'fs', right) if k < size - 1 else None  52.7 us
    psum x1, blocking collectives, per_device(): totals = lax.psum(local_sums, ('fs', 'tp'))  39.7 us
    unnamed x29, local copies, waits for them, and re-layouts  19.2 us
  transfers between devices with their start and end apart: 10, of which 8 were waited for; matrix products, arithmetic and copies ran while one was open for 10% of the time, Pallas kernels for 0%

profile of v1, /device:TPU:0, one launch (start us, length us, event | category | flops | bytes accessed | tf_op | source)
XLA Modules:
  0.0 313.8 jit_solution(17152881756715631259)
XLA Ops:
  7.2 1.8 copy.48
  9.1 3.0 collective-permute-start
  12.0 1.2 copy.41
  13.7 1.2 copy.44
  15.0 23.8 %while.12 = (s32[]{:T(128)}, bf16[4,384,128]{1,2,0:T(8,128)(2,1)}, bf16[4,384,128]{2,1,0:T(8,128)(2,1)}, bf16[4,384,2,64]{1,3,2,0:T(8,128)(2,1)S(1)}, bf16[4,384...) while((s32[]{:T(128)}, bf16[4,384,128]{1,2,0:T(8,128)(2,1)}, ...), condition=%wide.region_9.10_spmd, body=%wide.region_0.9_spmd.sunk | while | flops 195525504 | bytes 10978449 | solution.py:73
  17.1 0.8 subtract_convert_fusion.5
  18.2 1.0 fusion.101
  20.3 0.7 constant_dynamic-update-slice_fusion.2
  23.1 0.8 subtract_convert_fusion.5
  24.2 1.0 fusion.101
  29.0 0.8 subtract_convert_fusion.5
  30.1 1.0 fusion.101
  34.9 0.8 subtract_convert_fusion.5
  36.0 1.0 fusion.101
  38.7 1.2 copy.47
  40.3 1.6 collective-permute-start.1
  41.9 1.2 convolution_add_fusion.7
  43.1 7.9 %collective-permute-done.1 = bf16[256,2,256]{2,0,1:T(8,128)(2,1)S(1)} collective-permute-done((bf16[256,2,256]{2,0,1:T(8,128)(2,1)}, bf16[256,2,256]{2,0,1:T(8,128)(2,1)S(1)}, u32[]{:S(2)}, u32[]{:S(2)}) %collective-permute-start.1) | collective-permute-done | bytes 262176 | tf_op jit(solution)/shard_map/ppermute | solution.py:88
  51.3 9.3 %collective-permute-done.2 = bf16[256,2,256]{2,0,1:T(8,128)(2,1)S(1)} collective-permute-done((bf16[256,2,256]{2,0,1:T(8,128)(2,1)S(1)}, bf16[256,2,256]{2,0,1:T(8,128)(2,1)S(1)}, u32[]{:S(2)}, u32[]{:S(2)}) %collective-permute-start.2) | collective-permute-done | bytes 262176 | tf_op jit(solution)/shard_map/ppermute | solution.py:88
  60.9 8.8 %collective-permute-done.3 = bf16[256,2,256]{2,0,1:T(8,128)(2,1)S(1)} collective-permute-done((bf16[256,2,256]{2,0,1:T(8,128)(2,1)S(1)}, bf16[256,2,256]{2,0,1:T(8,128)(2,1)S(1)}, u32[]{:S(2)}, u32[]{:S(2)}) %collective-permute-start.3) | collective-permute-done | bytes 262176 | tf_op jit(solution)/shard_map/ppermute | solution.py:88
  70.0 8.8 %collective-permute-done.4 = bf16[256,2,256]{2,0,1:T(8,128)(2,1)S(1)} collective-permute-done((bf16[256,2,256]{2,0,1:T(8,128)(2,1)S(1)}, bf16[256,2,256]{2,0,1:T(8,128)(2,1)S(1)}, u32[]{:S(2)}, u32[]{:S(2)}) %collective-permute-start.4) | collective-permute-done | bytes 262176 | tf_op jit(solution)/shard_map/ppermute | solution.py:88
  79.1 9.1 %collective-permute-done.5 = bf16[256,2,256]{2,0,1:T(8,128)(2,1)S(1)} collective-permute-done((bf16[256,2,256]{2,0,1:T(8,128)(2,1)S(1)}, bf16[256,2,256]{2,0,1:T(8,128)(2,1)S(1)}, u32[]{:S(2)}, u32[]{:S(2)}) %collective-permute-start.5) | collective-permute-done | bytes 262176 | tf_op jit(solution)/shard_map/ppermute | solution.py:88
  88.4 8.8 %collective-permute-done.6 = bf16[256,2,256]{2,0,1:T(8,128)(2,1)S(1)} collective-permute-done((bf16[256,2,256]{2,0,1:T(8,128)(2,1)S(1)}, bf16[256,2,256]{2,0,1:T(8,128)(2,1)S(1)}, u32[]{:S(2)}, u32[]{:S(2)}) %collective-permute-start.6) | collective-permute-done | bytes 262176 | tf_op jit(solution)/shard_map/ppermute | solution.py:88
  98.4 1.3 copy.50
  101.0 74.3 %all-reduce.3.cloned.1.call-done = f32[256,2,512]{2,1,0:T(2,128)} async-done(((f32[256,2,512]{2,1,0:T(2,128)}), f32[256,2,512]{2,1,0:T(2,128)}) %all-reduce.3.cloned.1.call-update) | async-done | bytes 1048592
  175.4 1.8 multiply_reduce_fusion.3
  177.3 1.4 copy.53
  178.7 39.7 %psum.7 = f32[2]{0:T(128)S(1)} all-reduce(f32[2]{0:T(128)S(1)} %get-tuple-element.111), channel_id=1, replica_groups=mesh['fs'=8,'tp'=4] {'fs','tp'}, use_global_device_ids=true, to_apply=%region_12.13 | all-reduce | flops 2 | bytes 16 | tf_op jit(solution)/shard_map/psum | solution.py:109
  218.4 3.5 %subtract_convert_fusion.1 = (bf16[256,2,512]{0,2,1:T(8,128)(2,1)}, f32[256,2,512]{0,2,1:T(8,128)S(1)}) fusion(f32[256,2,512]{0,2,1:T(8,128)} %copy.53, f32[2]{0:T(128)S(1)} %rsqrt_multiply_fusion, bf16[256,2,256]{2,1,0:T(2,128)(2,1)S(1)} %copy-done.1, f32[256,2,512]{2,1,0:T(2,128)} %all-gather.3.cloned.1.call-done), kind=kOutput, calls=%fused_computation.66 | convolution fusion | flops 806092800 | bytes 3932168 | tf_op jit(solution)/shard_map/dkr,rke->dke/dot_general | solution.py:112
  221.9 1.3 copy.54
  223.2 72.9 %all-gather.5.cloned.1.call-done = bf16[2048,2,512]{0,2,1:T(8,128)(2,1)} async-done(((bf16[256,2,512]{0,2,1:T(8,128)(2,1)}), bf16[2048,2,512]{0,2,1:T(8,128)(2,1)}) %all-gather.5.cloned.1.call-update) | async-done | bytes 4194320 | tf_op jit(solution)/shard_map/all_gather | solution.py:119
  296.1 11.1 %copy.55 = bf16[2048,2,512]{2,1,0:T(2,128)(2,1)} copy(bf16[2048,2,512]{0,2,1:T(8,128)(2,1)} %all-gather.5.cloned.1.call-done) | data formatting | bytes 8388608
  (103 shorter events, 17.1 us)
Async XLA Ops:
  7.2 32.8 %copy-start = (bf16[384,2048]{1,0:T(8,128)(2,1)S(1)}, bf16[384,2048]{1,0:T(8,128)(2,1)}, u32[]{:S(2)}) copy-start(bf16[384,2048]{1,0:T(8,128)(2,1)} %param.12) | copy-start | bytes 4718596
  7.2 6.1 %copy-start.4 = (bf16[384,512]{1,0:T(8,128)(2,1)S(1)}, bf16[384,512]{1,0:T(8,128)(2,1)}, u32[]{:S(2)}) copy-start(bf16[384,512]{1,0:T(8,128)(2,1)} %param.14) | copy-start | bytes 1179652
  7.2 6.3 %copy-start.5 = (bf16[384,512]{1,0:T(8,128)(2,1)S(1)}, bf16[384,512]{1,0:T(8,128)(2,1)}, u32[]{:S(2)}) copy-start(bf16[384,512]{1,0:T(8,128)(2,1)} %param.15) | copy-start | bytes 1179652
  7.2 168.2 %all-reduce.3.cloned.1.call-start = ((), (), s32[]{:S(2)}) async-start(), calls=%async_computation.2 | async-start | bytes 2097152
  9.1 31.2 %collective-permute-start = (bf16[256,2,256]{2,0,1:T(8,128)(2,1)}, bf16[256,2,256]{2,0,1:T(8,128)(2,1)}, u32[]{:S(2)}, u32[]{:S(2)}) collective-permute-start(bf16[256,2,256]{2,0,1:T(8,128)(2,1)} %copy.48), channel_id=1, source_target_pairs={{0,4},{4,8},{8,12},{12,16},{16,20},{20,24},{24,28},{28,0},{1,5},{5... | collective-permute-start | bytes 786440 | tf_op jit(solution)/shard_map/ppermute | solution.py:88
  12.0 2.9 copy-start.7
  12.0 2.9 copy-start.8
  15.0 25.0 %copy-start.1 = (bf16[256,2,256]{2,1,0:T(2,128)(2,1)S(1)}, bf16[256,2,256]{2,1,0:T(2,128)(2,1)}, u32[]{:S(2)}) copy-start(bf16[256,2,256]{2,1,0:T(2,128)(2,1)} %param.19) | copy-start | bytes 786436
  40.3 10.7 %collective-permute-start.1 = (bf16[256,2,256]{2,0,1:T(8,128)(2,1)}, bf16[256,2,256]{2,0,1:T(8,128)(2,1)S(1)}, u32[]{:S(2)}, u32[]{:S(2)}) collective-permute-start(bf16[256,2,256]{2,0,1:T(8,128)(2,1)} %collective-permute-done), channel_id=1, source_target_pairs={{0,4},{4,8},{8,12},{12,16},{16,20},{20,24},{24,28},{28,0},{1,5},{5... | collective-permute-start | bytes 786440 | tf_op jit(solution)/shard_map/ppermute | solution.py:88
  51.0 9.6 %collective-permute-start.2 = (bf16[256,2,256]{2,0,1:T(8,128)(2,1)S(1)}, bf16[256,2,256]{2,0,1:T(8,128)(2,1)S(1)}, u32[]{:S(2)}, u32[]{:S(2)}) collective-permute-start(bf16[256,2,256]{2,0,1:T(8,128)(2,1)S(1)} %collective-permute-done.1), channel_id=1, source_target_pairs={{0,4},{4,8},{8,12},{12,16},{16,20},{20,24},{24,28},{28,0},{1,5},{5... | collective-permute-start | bytes 786440 | tf_op jit(solution)/shard_map/ppermute | solution.py:88
  60.6 9.1 %collective-permute-start.3 = (bf16[256,2,256]{2,0,1:T(8,128)(2,1)S(1)}, bf16[256,2,256]{2,0,1:T(8,128)(2,1)S(1)}, u32[]{:S(2)}, u32[]{:S(2)}) collective-permute-start(bf16[256,2,256]{2,0,1:T(8,128)(2,1)S(1)} %collective-permute-done.2), channel_id=1, source_target_pairs={{0,4},{4,8},{8,12},{12,16},{16,20},{20,24},{24,28},{28,0},{1,5},{5... | collective-permute-start | bytes 786440 | tf_op jit(solution)/shard_map/ppermute | solution.py:88
  69.7 9.1 %collective-permute-start.4 = (bf16[256,2,256]{2,0,1:T(8,128)(2,1)S(1)}, bf16[256,2,256]{2,0,1:T(8,128)(2,1)S(1)}, u32[]{:S(2)}, u32[]{:S(2)}) collective-permute-start(bf16[256,2,256]{2,0,1:T(8,128)(2,1)S(1)} %collective-permute-done.3), channel_id=1, source_target_pairs={{0,4},{4,8},{8,12},{12,16},{16,20},{20,24},{24,28},{28,0},{1,5},{5... | collective-permute-start | bytes 786440 | tf_op jit(solution)/shard_map/ppermute | solution.py:88
  78.8 9.4 %collective-permute-start.5 = (bf16[256,2,256]{2,0,1:T(8,128)(2,1)S(1)}, bf16[256,2,256]{2,0,1:T(8,128)(2,1)S(1)}, u32[]{:S(2)}, u32[]{:S(2)}) collective-permute-start(bf16[256,2,256]{2,0,1:T(8,128)(2,1)S(1)} %collective-permute-done.4), channel_id=1, source_target_pairs={{0,4},{4,8},{8,12},{12,16},{16,20},{20,24},{24,28},{28,0},{1,5},{5... | collective-permute-start | bytes 786440 | tf_op jit(solution)/shard_map/ppermute | solution.py:88
  79.0 18.4 %copy-start.2 = (bf16[4,384,128]{1,2,0:T(8,128)(2,1)S(1)}, bf16[4,384,128]{1,2,0:T(8,128)(2,1)}, u32[]{:S(2)}) copy-start(bf16[4,384,128]{1,2,0:T(8,128)(2,1)} %get-tuple-element.51) | copy-start | bytes 1179652
  88.2 9.1 %collective-permute-start.6 = (bf16[256,2,256]{2,0,1:T(8,128)(2,1)S(1)}, bf16[256,2,256]{2,0,1:T(8,128)(2,1)S(1)}, u32[]{:S(2)}, u32[]{:S(2)}) collective-permute-start(bf16[256,2,256]{2,0,1:T(8,128)(2,1)S(1)} %collective-permute-done.5), channel_id=1, source_target_pairs={{0,4},{4,8},{8,12},{12,16},{16,20},{20,24},{24,28},{28,0},{1,5},{5... | collective-permute-start | bytes 786440 | tf_op jit(solution)/shard_map/ppermute | solution.py:88
  98.4 1.4 copy-start.9
  98.4 77.0 %copy-start.6 = (f32[32,2,512]{2,1,0:T(2,128)S(1)}, f32[32,2,512]{2,1,0:T(2,128)}, u32[]{:S(2)}) copy-start(f32[32,2,512]{2,1,0:T(2,128)} %param.20) | copy-start | bytes 393220
  99.7 77.5 %copy-start.3 = (f32[256,2,512]{2,1,0:T(2,128)S(1)}, f32[256,2,512]{2,1,0:T(2,128)}, u32[]{:S(2)}) copy-start(f32[256,2,512]{2,1,0:T(2,128)} %param.21) | copy-start | bytes 3145732
  99.7 118.7 %all-gather.3.cloned.1.call-start = ((), (), s32[]{:S(2)}) async-start(), calls=%async_computation | async-start | bytes 1179648 | tf_op jit(solution)/shard_map/all_gather | solution.py:115
  177.2 118.9 %all-gather.5.cloned.1.call-start = ((), (), s32[]{:S(2)}) async-start(), calls=%async_computation.1 | async-start | bytes 4718592 | tf_op jit(solution)/shard_map/all_gather | solution.py:119
Sparse Core Ops, SparseCore 0:
  99.9 75.4 all-reduce.2
  178.1 40.0 all-gather.2
  222.0 74.0 all-gather.4
